TPU v7x, 256 devices: a whole 4x4x8 slice. The times are simulated.
256 devices in a mesh: kv: 32 (over z, x), tp: 8 (over y, core).
Axes of the slice: x: 4, y: 4, z: 8, core: 2. Of those that a mesh axis runs over, the one named last changes fastest.
Arguments:
- tokens: bfloat16 [22, 4096], P(None, ('kv', 'tp')), may hold values from -22 to 22
- attn_gain: float32 [4096], P('kv'), may hold values from 0.1 to 1.9
- w_query: bfloat16 [4096, 4096], P('kv', 'tp'), may hold values from -0.09375 to 0.09375
- w_key: bfloat16 [4096, 4096], P('kv', 'tp'), may hold values from -0.5 to 0.5
- w_value: bfloat16 [4096, 4096], P('kv', 'tp'), may hold values from -0.09375 to 0.09375
- cache_keys: bfloat16 [22, 8192, 32, 128], P(None, 'kv', 'tp'), may hold values from -256 to 256
- cache_values: bfloat16 [22, 8192, 32, 128], P(None, 'kv', 'tp'), may hold values from -6 to 6
- lambdas: float32 [32], P('tp'), may hold values from 0.3 to 0.8
- head_gain: float32 [128], replicated, may hold values from 0.1 to 1.9
- w_out: bfloat16 [4096, 4096], P('tp', 'kv'), may hold values from -0.09375 to 0.09375
- mlp_gain: float32 [4096], P('kv'), may hold values from 0.1 to 1.9
- w_gate: bfloat16 [4096, 11008], P('kv', 'tp'), may hold values from -0.09375 to 0.09375
- w_up: bfloat16 [4096, 11008], P('kv', 'tp'), may hold values from -0.09375 to 0.09375
- w_down: bfloat16 [11008, 4096], P('tp', 'kv'), may hold values from -0.0546875 to 0.0546875
Outputs:
- output: bfloat16 [22, 4096], P(None, ('kv', 'tp'))
All inputs are finite; a program needn't handle non-finite values.
Results may differ from a plain program's by a relative error of at most 0.017.
The roundings to bfloat16 on the way count: a program that leaves them out, or rounds other values in their place, can miss the bound.
Values may be sent and summed in bfloat16 or wider, within the bound.
A program may use at most 64 MiB of HBM per device.

v0:
```python
import jax
import jax.numpy as jnp
from jax import lax
from jax.sharding import Mesh
from jax.sharding import PartitionSpec as P

D = 4096
KV = ("kv_0", "kv_1")
KV_TP = ("kv_0", "kv_1", "tp")


epsilon = 1e-06


def from_everyone(shard, axis):
    copies = jnp.broadcast_to(shard, (lax.axis_size(axis), *shard.shape))
    return lax.all_to_all(copies, axis, split_axis=0, concat_axis=0, tiled=True)


def joined_along(tiles, dim):
    tiles = jnp.moveaxis(tiles, 0, dim)
    lengths = tiles.shape
    return tiles.reshape(*lengths[:dim], lengths[dim] * lengths[dim + 1], *lengths[dim + 2 :])


def collect(shard, axis, dim):
    tiles = from_everyone(shard, axis)
    return joined_along(tiles, dim)


def rows_for(lines, size):
    spare = -lines.shape[0] % size
    if not spare:
        return lines
    return jnp.concatenate([lines, jnp.zeros((spare, *lines.shape[1:]), lines.dtype)])


def split_up(shard, dim, size):
    lengths = shard.shape
    tiles = shard.reshape(*lengths[:dim], size, lengths[dim] // size, *lengths[dim + 1 :])
    return jnp.moveaxis(tiles, dim, 0)


def sum_at_owner(shard, axis, dim):
    size = lax.axis_size(axis)
    tiles = lax.all_to_all(split_up(shard, dim, size), axis, 0, 0, tiled=True)
    return jnp.sum(tiles, axis=0)


def nested_sum(shard, axes):
    padded = rows_for(shard, lax.axis_size(axes))
    whole = collect(sum_at_owner(padded, axes, 0), axes, 0)
    return lax.slice_in_dim(whole, 0, len(shard)).reshape(shard.shape)


def packed_total(arrays, axis):
    ravelled, at, done = (jnp.concatenate([a.reshape(-1) for a in arrays]), 0, [])
    running = nested_sum(ravelled, axis)
    for a in arrays:
        done.append(running[at : at + a.size].reshape(a.shape))
        at += a.size
    return tuple(done)


def all_in_one(shard, axis):
    leaves = jax.tree.leaves(shard)
    turns = sorted(range(len(leaves)), key=lambda k: -leaves[k].size)
    width = (1, *leaves[turns[0]].shape)[-1]
    lines = [
        jnp.pad(leaves[k].reshape(-1), (0, -leaves[k].size % width)).reshape(-1, width)
        for k in turns
    ]
    both, at, found = (lax.all_gather(jnp.concatenate(lines), axis), 0, {})
    for k, line in zip(turns, lines):
        section = both[:, at : at + len(line)].reshape(len(both), -1)
        found[k] = section[:, : leaves[k].size].reshape(-1, *leaves[k].shape)
        at += len(line)
    numbers = iter(range(len(leaves)))
    return jax.tree.map(lambda _: found[next(numbers)], shard)


def joined_all(shard, axes, combine):
    for axis in axes:
        pieces = all_in_one(shard, axis)
        shard = jax.tree.map(lambda part: part[0], pieces)
        for k in range(1, lax.axis_size(axis)):
            shard = combine(shard, jax.tree.map(lambda part: part[k], pieces))
    return shard


def taken_together(shard, axis):
    everything = from_everyone(shard, axis)
    return jnp.sum(everything.astype(jnp.float32), axis=0)


def taken_together_2(shard, axis):
    everything = from_everyone(shard, axis)
    return jnp.sum(everything, axis=0)


def summed_on_arrival(shard, axis, dim):
    tiles = split_up(shard, dim, lax.axis_size(axis))
    arrived = lax.all_to_all(tiles, axis, split_axis=0, concat_axis=0, tiled=True)
    return arrived.astype(jnp.float32).sum(axis=0)


def join_map(left_max, left_sum, left_val, right_max, right_sum, right_val):
    peak_val = jnp.maximum(left_max, right_max)
    left_weight = jnp.exp(left_max - peak_val)
    right_weight = jnp.exp(right_max - peak_val)
    return (
        peak_val,
        left_sum * left_weight + right_sum * right_weight,
        left_val * left_weight[..., None] + right_val * right_weight[..., None],
    )


def combine(earlier, later):
    return join_map(earlier[0], earlier[1], earlier[2], later[0], later[1], later[2]) + join_map(
        earlier[3], earlier[4], earlier[5], later[3], later[4], later[5]
    )


def per_device(
    tokens,
    attn_gain,
    w_query,
    w_key,
    w_value,
    cache_keys,
    cache_values,
    lambdas,
    head_gain,
    w_out,
    mlp_gain,
    w_gate,
    w_up,
    w_down,
):
    seq_count = tokens.shape[0]
    own_width = tokens.shape[1]
    local_heads = lambdas.shape[0]
    head_dim = head_gain.shape[0]
    half_dim = head_dim // 2
    score_scale = half_dim ** (-0.5)
    gathered = collect(tokens, "tp", 1)
    gathered_f = gathered.astype(jnp.float32)
    normed_in = (gathered_f * attn_gain).astype(jnp.bfloat16)
    query_part = jnp.dot(normed_in, w_query, preferred_element_type=jnp.float32)
    key_part = jnp.dot(normed_in, w_key, preferred_element_type=jnp.float32)
    value_part = jnp.dot(normed_in, w_value, preferred_element_type=jnp.float32)
    query_sum, key_sum, value_sum, square_sum = packed_total(
        (query_part, key_part, value_part, jnp.sum(gathered_f * gathered_f, axis=1, keepdims=True)),
        KV,
    )
    scale_in = lax.rsqrt(square_sum / D + epsilon)
    query_rows = (
        (scale_in * query_sum).astype(jnp.bfloat16).reshape(seq_count, local_heads, head_dim)
    )
    key_new = (scale_in * key_sum).astype(jnp.bfloat16).reshape(seq_count, local_heads, head_dim)
    value_new = (
        (scale_in * value_sum).astype(jnp.bfloat16).reshape(seq_count, local_heads, head_dim)
    )

    def partial_map(low, high):
        scores = (
            jnp.einsum(
                "shd,sthd->sht",
                query_rows[:, :, low:high],
                cache_keys[:, :, :, low:high],
                preferred_element_type=jnp.float32,
            )
            * score_scale
        )
        maxima = jnp.max(scores, axis=2)
        weights = jnp.exp(scores - maxima[:, :, None])
        totals = jnp.sum(weights, axis=2)
        summed = jnp.einsum(
            "sht,sthd->shd",
            weights.astype(jnp.bfloat16),
            cache_values,
            preferred_element_type=jnp.float32,
        )
        return (maxima, totals, summed)

    def own_term(low, high):
        score_new = (
            jnp.sum(
                query_rows[:, :, low:high].astype(jnp.float32)
                * key_new[:, :, low:high].astype(jnp.float32),
                axis=2,
            )
            * score_scale
        )
        return (score_new, jnp.ones_like(score_new), value_new.astype(jnp.float32))

    first_part = partial_map(0, half_dim)
    second_part = partial_map(half_dim, head_dim)
    merged = joined_all(
        (
            first_part[0],
            first_part[1],
            first_part[2],
            second_part[0],
            second_part[1],
            second_part[2],
        ),
        KV,
        combine,
    )
    combined = combine(merged, own_term(0, half_dim) + own_term(half_dim, head_dim))
    first_map = combined[2] / combined[1][:, :, None]
    second_map = combined[5] / combined[4][:, :, None]
    difference = first_map - lambdas[None, :, None] * second_map
    normed = (
        difference
        * lax.rsqrt(jnp.mean(difference * difference, axis=2, keepdims=True) + epsilon)
        * head_gain
    )
    heads_out = normed.astype(jnp.bfloat16).reshape(seq_count, local_heads * head_dim)
    branch = taken_together(
        jnp.dot(heads_out, w_out, preferred_element_type=jnp.float32).astype(jnp.bfloat16), "tp"
    ).astype(jnp.float32)
    residual = (gathered_f + branch).astype(jnp.bfloat16)
    residual_f = residual.astype(jnp.float32)
    mid_sum = taken_together_2(jnp.sum(residual_f * residual_f, axis=1, keepdims=True), KV)
    scale_mid = lax.rsqrt(mid_sum / D + epsilon)
    normed_mid = (residual_f * mlp_gain).astype(jnp.bfloat16)
    gate_part = jnp.dot(normed_mid, w_gate, preferred_element_type=jnp.float32)
    up_part = jnp.dot(normed_mid, w_up, preferred_element_type=jnp.float32)
    gate_sum, up_sum = packed_total((gate_part, up_part), KV)
    hidden = (jax.nn.silu(scale_mid * gate_sum) * (scale_mid * up_sum)).astype(jnp.bfloat16)
    down_part = jnp.dot(hidden, w_down, preferred_element_type=jnp.float32).astype(jnp.bfloat16)
    mixer_own = summed_on_arrival(down_part, "tp", 1)
    tp_index = lax.axis_index("tp")
    residual_own = lax.dynamic_slice_in_dim(residual_f, tp_index * own_width, own_width, 1)
    return (residual_own + mixer_own).astype(jnp.bfloat16)


def solution(mesh):
    split = Mesh(mesh.devices.reshape(8, 4, mesh.shape["tp"]), ("kv_0", "kv_1", "tp"))
    placed = (
        P(None, KV_TP),
        P(KV),
        P(KV, "tp"),
        P(KV, "tp"),
        P(KV, "tp"),
        P(None, KV, "tp", None),
        P(None, KV, "tp", None),
        P("tp"),
        P(),
        P("tp", KV),
        P(KV),
        P(KV, "tp"),
        P(KV, "tp"),
        P("tp", KV),
    )
    return jax.shard_map(
        per_device, mesh=split, in_specs=placed, out_specs=P(None, KV_TP), check_vma=False
    )
```

profile of v0, /device:TPU:1, one launch (start us, length us, event | category | flops | bytes accessed | tf_op | source)
XLA Modules:
  0.0 190.5 jit_solution(10570585366139509377)
XLA Ops:
  0.0 0.7 broadcast_bitcast_fusion.2
  0.9 10.4 %all_to_all.50 = bf16[8,2,176]{2,1,0:T(2,128)(2,1)S(1)} all-to-all(bf16[8,2,176]{2,1,0:T(2,128)(2,1)S(1)} %reshape.1755), channel_id=1, replica_groups=mesh['kv_0'=8,'kv_1'=4,'tp'=8] {'tp'}, dimensions={0} | all-to-all | bytes 11264 | tf_op jit(solution)/shard_map/all_to_all | solution.py:17
  11.4 0.7 multiply_convert_fusion.6
  12.1 1.0 fusion.202
  13.2 1.0 fusion.201
  14.2 1.0 fusion.200
  15.6 20.3 %all_to_all.51 = f32[32,1,1057]{2,1,0:T(1,128)S(1)} all-to-all(f32[32,1,1057]{2,1,0:T(1,128)S(1)} %all_to_all.33), channel_id=1, replica_groups=mesh['kv_0'=8,'kv_1'=4,'tp'=8] {'kv_0','kv_1'}, dimensions={0} | all-to-all | bytes 270592 | tf_op jit(solution)/shard_map/all_to_all | solution.py:46
  36.0 0.7 broadcast_in_dim.11
  36.8 3.9 %all-to-all-start.2 = ((f32[32,1,1057]{2,1,0:T(1,128)}), f32[32,1,1057]{2,1,0:T(1,128)S(1)}, u32[]{:S(2)}, u32[]{:S(2)}) async-start(f32[32,1,1057]{2,1,0:T(1,128)} %broadcast_in_dim.11), calls=%async_computation.2 | async-start | bytes 294912 | tf_op jit(solution)/shard_map/all_to_all | solution.py:17
  40.7 12.1 %fusion.195 = (bf16[22,256,4,64]{3,2,1,0:T(4,128)(2,1)}, bf16[22,256,4,64]{3,2,1,0:T(4,128)(2,1)}) fusion(bf16[22,256,4,128]{3,2,1,0:T(4,128)(2,1)} %param.19), kind=kLoop, calls=%fused_computation.348 | loop fusion | bytes 11534336 | tf_op jit(solution)/shard_map/slice | solution.py:170
  53.6 4.2 %fusion = f32[22,4,1,256]{3,2,1,0:T(1,128)S(1)} fusion(bf16[22,256,4,64]{3,2,1,0:T(4,128)(2,1)} %get-tuple-element.103, bf16[22,4,64,1]{2,1,0,3:T(4,128)(2,1)S(1)} %get-tuple-element.128), kind=kOutput, calls=%fused_computation | convolution fusion | flops 2883584 | bytes 2984960 | tf_op jit(solution)/shard_map/shd,sthd->sht/dot_general | solution.py:167
  58.3 4.2 %fusion.2 = f32[22,4,1,256]{3,2,1,0:T(1,128)S(1)} fusion(bf16[22,256,4,64]{3,2,1,0:T(4,128)(2,1)} %get-tuple-element.104, bf16[22,4,64,1]{2,1,0,3:T(4,128)(2,1)S(1)} %get-tuple-element.129), kind=kOutput, calls=%fused_computation.2 | convolution fusion | flops 2883584 | bytes 2984960 | tf_op jit(solution)/shard_map/shd,sthd->sht/dot_general | solution.py:167
  63.1 3.5 %fusion.4 = f32[22,4,1,128]{3,2,1,0:T(1,128)S(1)} fusion(bf16[22,256,4,128]{3,2,1,0:T(4,128)(2,1)} %param.20, bf16[22,4,256,1]{2,1,0,3:T(4,128)(2,1)S(1)} %get-tuple-element.125), kind=kOutput, calls=%fused_computation.4 | convolution fusion | flops 5767168 | bytes 5857280 | tf_op jit(solution)/shard_map/sht,sthd->shd/dot_general | solution.py:178
  66.6 3.5 %fusion.6 = f32[22,4,1,128]{3,2,1,0:T(1,128)S(1)} fusion(bf16[22,256,4,128]{3,2,1,0:T(4,128)(2,1)} %param.20, bf16[22,4,256,1]{2,1,0,3:T(4,128)(2,1)S(1)} %get-tuple-element.127), kind=kOutput, calls=%fused_computation.6 | convolution fusion | flops 5767168 | bytes 5857280 | tf_op jit(solution)/shard_map/sht,sthd->shd/dot_general | solution.py:178
  70.1 21.7 %all-gather.2 = f32[8,180,128]{2,1,0:T(8,128)S(1)} all-gather(f32[1,180,128]{2,1,0:T(8,128)S(1)} %bitcast.717), channel_id=2, replica_groups=mesh['kv_0'=8,'kv_1'=4,'tp'=8] {'kv_0'}, dimensions={0}, use_global_device_ids=true | all-gather | bytes 829440 | tf_op jit(solution)/shard_map/all_gather | solution.py:73
  92.5 10.2 %all-gather.3 = f32[4,180,128]{2,1,0:T(8,128)S(1)} all-gather(f32[1,180,128]{2,1,0:T(8,128)S(1)} %bitcast.716), channel_id=3, replica_groups=mesh['kv_0'=8,'kv_1'=4,'tp'=8] {'kv_1'}, dimensions={0}, use_global_device_ids=true | all-gather | bytes 460800 | tf_op jit(solution)/shard_map/all_gather | solution.py:73
  105.1 0.4 fusion.83
  108.3 17.9 %all_to_all.52 = bf16[8,22,128]{2,1,0:T(8,128)(2,1)S(1)} all-to-all(bf16[8,22,128]{2,1,0:T(8,128)(2,1)S(1)} %broadcast_in_dim.12), channel_id=1, replica_groups=mesh['kv_0'=8,'kv_1'=4,'tp'=8] {'tp'}, dimensions={0} | all-to-all | bytes 90112 | tf_op jit(solution)/shard_map/all_to_all | solution.py:17
  127.2 0.8 all_to_all.38
  128.0 7.4 %all-to-all-start.5 = ((f32[32,1,1892]{2,1,0:T(1,128)}), f32[32,1,1892]{2,1,0:T(1,128)S(1)}, u32[]{:S(2)}, u32[]{:S(2)}) async-start(f32[32,1,1892]{2,1,0:T(1,128)} %all_to_all.38), calls=%async_computation.5 | async-start | bytes 491520 | tf_op jit(solution)/shard_map/all_to_all | solution.py:46
  135.6 10.8 %all-to-all-done.5 = f32[32,1,1892]{2,1,0:T(1,128)S(1)} async-done(((f32[32,1,1892]{2,1,0:T(1,128)}), f32[32,1,1892]{2,1,0:T(1,128)S(1)}, u32[]{:S(2)}, u32[]{:S(2)}) %all-to-all-start.5) | async-done | bytes 242208 | tf_op jit(solution)/shard_map/all_to_all | solution.py:46
  146.4 0.6 broadcast_in_dim.13
  147.0 4.7 %all-to-all-start.4 = ((f32[32,22,1]{1,2,0:T(1,128)}), f32[32,22,1]{1,2,0:T(1,128)S(1)}, u32[]{:S(2)}, u32[]{:S(2)}) async-start(f32[32,22,1]{1,2,0:T(1,128)} %broadcast_in_dim.13), calls=%async_computation.4 | async-start | bytes 32768 | tf_op jit(solution)/shard_map/all_to_all | solution.py:17
  151.9 8.5 %all-to-all-done.4 = f32[32,22,1]{1,2,0:T(1,128)S(1)} async-done(((f32[32,22,1]{1,2,0:T(1,128)}), f32[32,22,1]{1,2,0:T(1,128)S(1)}, u32[]{:S(2)}, u32[]{:S(2)}) %all-to-all-start.4) | async-done | bytes 2848 | tf_op jit(solution)/shard_map/all_to_all | solution.py:17
  160.4 0.8 broadcast_in_dim.14
  161.2 3.9 %all-to-all-start.6 = ((f32[32,1,1892]{2,1,0:T(1,128)}), f32[32,1,1892]{2,1,0:T(1,128)S(1)}, u32[]{:S(2)}, u32[]{:S(2)}) async-start(f32[32,1,1892]{2,1,0:T(1,128)} %broadcast_in_dim.14), calls=%async_computation.6 | async-start | bytes 491520 | tf_op jit(solution)/shard_map/all_to_all | solution.py:17
  165.1 10.4 %all-to-all-done.6 = f32[32,1,1892]{2,1,0:T(1,128)S(1)} async-done(((f32[32,1,1892]{2,1,0:T(1,128)}), f32[32,1,1892]{2,1,0:T(1,128)S(1)}, u32[]{:S(2)}, u32[]{:S(2)}) %all-to-all-start.6) | async-done | bytes 242208 | tf_op jit(solution)/shard_map/all_to_all | solution.py:17
  175.5 0.7 slice_reduce_fusion.1
  177.0 0.7 reshape.1757
  177.7 7.2 %all-to-all-start.7 = ((bf16[8,2,176]{2,1,0:T(2,128)(2,1)}), bf16[8,2,176]{2,1,0:T(2,128)(2,1)S(1)}, u32[]{:S(2)}, u32[]{:S(2)}) async-start(bf16[8,2,176]{2,1,0:T(2,128)(2,1)} %reshape.1757), calls=%async_computation.7 | async-start | bytes 16384 | tf_op jit(solution)/shard_map/all_to_all | solution.py:103
  184.9 4.6 %all-to-all-done.7 = bf16[8,2,176]{2,1,0:T(2,128)(2,1)S(1)} async-done(((bf16[8,2,176]{2,1,0:T(2,128)(2,1)}), bf16[8,2,176]{2,1,0:T(2,128)(2,1)S(1)}, u32[]{:S(2)}, u32[]{:S(2)}) %all-to-all-start.7) | async-done | bytes 5664 | tf_op jit(solution)/shard_map/all_to_all | solution.py:103
  189.8 0.7 copy.43
  (183 shorter events, 10.1 us)
Async XLA Ops:
  0.0 126.2 %copy-start = (bf16[128,1376]{0,1:T(8,128)(2,1)S(1)}, bf16[128,1376]{0,1:T(8,128)(2,1)}, u32[]{:S(2)}) copy-start(bf16[128,1376]{0,1:T(8,128)(2,1)} %param.26) | copy-start | bytes 1056772
  36.8 16.1 %all-to-all-start.2 = ((f32[32,1,1057]{2,1,0:T(1,128)}), f32[32,1,1057]{2,1,0:T(1,128)S(1)}, u32[]{:S(2)}, u32[]{:S(2)}) async-start(f32[32,1,1057]{2,1,0:T(1,128)} %broadcast_in_dim.11), calls=%async_computation.2 | async-start | bytes 294912 | tf_op jit(solution)/shard_map/all_to_all | solution.py:17
  40.6 12.1 %copy-start.4 = (f32[4]{0:T(128)S(1)}, f32[4]{0:T(128)}, u32[]{:S(2)}) copy-start(f32[4]{0:T(128)} %param.21) | copy-start | bytes 52
  40.6 12.2 %copy-start.5 = (f32[128]{0:T(128)S(1)}, f32[128]{0:T(128)}, u32[]{:S(2)}) copy-start(f32[128]{0:T(128)} %param.22) | copy-start | bytes 1540
  70.1 37.9 %copy-start.2 = (bf16[512,128]{1,0:T(8,128)(2,1)S(1)}, bf16[512,128]{1,0:T(8,128)(2,1)}, u32[]{:S(2)}) copy-start(bf16[512,128]{1,0:T(8,128)(2,1)} %param.23) | copy-start | bytes 393220
  91.8 34.4 %copy-start.3 = (f32[128]{0:T(128)S(1)}, f32[128]{0:T(128)}, u32[]{:S(2)}) copy-start(f32[128]{0:T(128)} %param.24) | copy-start | bytes 1540
  92.2 34.4 %copy-start.1 = (bf16[128,1376]{0,1:T(8,128)(2,1)S(1)}, bf16[128,1376]{0,1:T(8,128)(2,1)}, u32[]{:S(2)}) copy-start(bf16[128,1376]{0,1:T(8,128)(2,1)} %param.25) | copy-start | bytes 1056772
  106.0 70.4 %copy-start.6 = (bf16[1376,128]{1,0:T(8,128)(2,1)S(1)}, bf16[1376,128]{1,0:T(8,128)(2,1)}, u32[]{:S(2)}) copy-start(bf16[1376,128]{1,0:T(8,128)(2,1)} %param.27) | copy-start | bytes 1056772
  128.0 18.4 %all-to-all-start.5 = ((f32[32,1,1892]{2,1,0:T(1,128)}), f32[32,1,1892]{2,1,0:T(1,128)S(1)}, u32[]{:S(2)}, u32[]{:S(2)}) async-start(f32[32,1,1892]{2,1,0:T(1,128)} %all_to_all.38), calls=%async_computation.5 | async-start | bytes 491520 | tf_op jit(solution)/shard_map/all_to_all | solution.py:46
  147.0 13.3 %all-to-all-start.4 = ((f32[32,22,1]{1,2,0:T(1,128)}), f32[32,22,1]{1,2,0:T(1,128)S(1)}, u32[]{:S(2)}, u32[]{:S(2)}) async-start(f32[32,22,1]{1,2,0:T(1,128)} %broadcast_in_dim.13), calls=%async_computation.4 | async-start | bytes 32768 | tf_op jit(solution)/shard_map/all_to_all | solution.py:17
  161.2 14.3 %all-to-all-start.6 = ((f32[32,1,1892]{2,1,0:T(1,128)}), f32[32,1,1892]{2,1,0:T(1,128)S(1)}, u32[]{:S(2)}, u32[]{:S(2)}) async-start(f32[32,1,1892]{2,1,0:T(1,128)} %broadcast_in_dim.14), calls=%async_computation.6 | async-start | bytes 491520 | tf_op jit(solution)/shard_map/all_to_all | solution.py:17
  177.7 11.8 %all-to-all-start.7 = ((bf16[8,2,176]{2,1,0:T(2,128)(2,1)}), bf16[8,2,176]{2,1,0:T(2,128)(2,1)S(1)}, u32[]{:S(2)}, u32[]{:S(2)}) async-start(bf16[8,2,176]{2,1,0:T(2,128)(2,1)} %reshape.1757), calls=%async_computation.7 | async-start | bytes 16384 | tf_op jit(solution)/shard_map/all_to_all | solution.py:103
where the time goes:
time: 191 us; the launch traced here: 190 us
  blocking collectives  80.4 us (42%)
  waiting for transfers between devices  34.3 us (18%)
  starting transfers between devices  27 us (14%)
  local copies, waits for them, and re-layouts  24.4 us (13%)
  matrix products  19.7 us (10%)
  other arithmetic  3.54 us (2%)
    all_gather x2, blocking collectives, all_in_one(): both, at, found = (lax.all_gather(jnp.concatenate(lines), axis), 0, {})  31.9 us
    all_to_all x2, blocking collectives, from_everyone(): return lax.all_to_all(copies, axis, split_axis=0, concat_axis=0, tiled=True)  28.2 us
    all_to_all x1, blocking collectives, sum_at_owner(): tiles = lax.all_to_all(split_up(shard, dim, size), axis, 0, 0, tiled=True)  20.3 us
    all_to_all x3, waiting for transfers between devices, from_everyone(): return lax.all_to_all(copies, axis, split_axis=0, concat_axis=0, tiled=True)  18.8 us
    all_to_all x3, starting transfers between devices, from_everyone(): return lax.all_to_all(copies, axis, split_axis=0, concat_axis=0, tiled=True)  12.4 us
    slice x1, local copies, waits for them, and re-layouts, partial_map(): cache_keys[:, :, :, low:high]  12.1 us
    all_to_all x1, waiting for transfers between devices, sum_at_owner(): tiles = lax.all_to_all(split_up(shard, dim, size), axis, 0, 0, tiled=True)  10.8 us
    dot_general x2, matrix products, partial_map(): jnp.einsum('shd,sthd->sht', query_rows[:, :, low:high], cache_keys[:, :,...  8.45 us
  transfers between devices with their start and end apart: 5, of which 4 were waited for; matrix products, arithmetic and copies ran while one was open for 7% of the time, Pallas kernels for 0%

commit v1 on v0

v1 whole, which is shorter than its diff:
```python
import functools

import jax
import jax.numpy as jnp
from jax import lax
from jax.experimental import pallas as pl
from jax.experimental.pallas import tpu as pltpu
from jax.sharding import PartitionSpec as P

MESH = pl.DeviceIdType.MESH
F32, BF16 = jnp.float32, jnp.bfloat16
D = 4096
EPS = 1e-06
ROWS = 24
SEQS = 22
N_KV, N_X, N_TP = 32, 4, 8
HEADS = 4
CHUNKS = 11
LOW = -3.0e38


def up(block):
    return block.astype(F32).reshape(block.shape[0] * 8, 128)


def tiles(rows):
    return rows.reshape(rows.shape[0] // 8, 8, 128).astype(BF16)


def iota(shape, dim):
    return lax.broadcasted_iota(jnp.int32, shape, dim)


def column_to_row(col):
    shape = (ROWS, 128)
    spread = jnp.where(iota(shape, 0) == iota(shape, 1), jnp.broadcast_to(col, shape), 0.0)
    return jnp.sum(spread, axis=0, keepdims=True)


def row_to_column(row):
    shape = (ROWS, 128)
    spread = jnp.where(iota(shape, 0) == iota(shape, 1), jnp.broadcast_to(row, shape), 0.0)
    return jnp.sum(spread, axis=1, keepdims=True)


def split_two(row):
    high = row.astype(BF16).astype(F32)
    return high, row - high


def with_rows(block, first, second):
    at = iota((ROWS, 128), 0)
    return jnp.where(at == SEQS, first, jnp.where(at == SEQS + 1, second, block))


def kernel(
    tok_hbm, again_hbm, wq_hbm, wk_hbm, wv_hbm, keys_hbm, vals_hbm, lam_hbm, hgain_hbm,
    wo_hbm, mgain_hbm, wg_hbm, wu_hbm, wd_hbm,
    out_ref,
    tok_v, again, wq, wk, wv, keys, vals, lam, hgain, wo, mgain, wg, wu, wd,
    x_all, x_rows,
    b_q, r_q, b_kv, r_kv, q_all, q_s, sc, o_s,
    b_o, r_o, m_s, l_s, h_all, r_b, res_t, b_g, r_g, hid, b_d, r_d,
    load_sem, send_sem, recv_sem,
):
    kv = lax.axis_index("kv")
    tp = lax.axis_index("tp")
    z = kv // N_X
    x = kv % N_X
    core = tp % 2

    def kv_peer(i):
        return ((z + i // N_X) % (N_KV // N_X)) * N_X + (x + i % N_X) % N_X

    def tp_peer(i):
        return (tp + i) % N_TP

    barrier = pltpu.get_barrier_semaphore()
    for i in range(1, N_TP):
        pl.semaphore_signal(barrier, inc=1, device_id=(kv, tp_peer(i)), device_id_type=MESH)
    for i in range(1, N_KV):
        pl.semaphore_signal(barrier, inc=1, device_id=(kv_peer(i), tp), device_id_type=MESH)

    loads = [
        pltpu.make_async_copy(src, dst, load_sem.at[n])
        for n, (src, dst) in enumerate(
            (
                (tok_hbm, tok_v), (again_hbm, again), (wq_hbm, wq), (wk_hbm, wk), (wv_hbm, wv),
                (keys_hbm, keys), (vals_hbm, vals), (lam_hbm, lam), (hgain_hbm, hgain),
                (wo_hbm, wo), (mgain_hbm, mgain), (wg_hbm, wg), (wu_hbm, wu),
                (wd_hbm, wd.at[pl.ds(0, wd_hbm.shape[0])]),
            )
        )
    ]
    for load in loads:
        load.start()
    (ld_tok, ld_again, ld_wq, ld_wk, ld_wv, ld_keys, ld_vals, ld_lam, ld_hgain, ld_wo, ld_mgain,
     ld_wg, ld_wu, ld_wd) = loads

    def copy_to(src, dst, phase, device):
        return pltpu.make_async_remote_copy(
            src_ref=src, dst_ref=dst, send_sem=send_sem.at[phase], recv_sem=recv_sem.at[phase],
            device_id=device, device_id_type=MESH,
        )

    def wait_bytes(ref, sem):
        pltpu.make_async_copy(ref, ref, sem).wait()

    wd[pl.ds(wd_hbm.shape[0], CHUNKS * 128 - wd_hbm.shape[0]), :] = jnp.zeros(
        (CHUNKS * 128 - wd_hbm.shape[0], 128), BF16
    )
    b_g[...] = jnp.zeros(b_g.shape, BF16)
    o_s[...] = jnp.zeros(o_s.shape, F32)
    for c in range(8):
        for s in range(SEQS, ROWS):
            sc[c, pl.ds(s, 8, stride=ROWS), :] = jnp.zeros((8, 128), F32)

    ld_tok.wait()
    x_all[tp] = jnp.concatenate(
        [tok_v[...].astype(F32), jnp.zeros((16, 128 - SEQS), F32)], axis=1
    ).astype(BF16)
    pl.semaphore_wait(barrier, N_TP - 1 + N_KV - 1)

    for i in range(1, N_TP):
        copy_to(x_all.at[tp], x_all.at[tp], 0, (kv, tp_peer(i))).start()
    ld_again.wait()
    ld_wq.wait()
    wait_bytes(x_all.at[pl.ds(0, N_TP - 1)], recv_sem.at[0])
    x_cols = x_all[...].astype(F32).reshape(128, 128)
    x_f = jnp.transpose(x_cols)[:ROWS]
    x_rows[...] = x_f
    normed = (x_f * again[...]).astype(BF16)
    square_row = column_to_row(jnp.sum(x_f * x_f, axis=1, keepdims=True))
    sq_high, sq_low = split_two(square_row)

    def head_owner(h):
        return 8 * h + 6 * core

    k_own = kv - 6 * core
    own_head = jnp.clip(k_own // 8, 0, HEADS - 1)
    is_head_owner = (kv == head_owner(own_head))

    q_part = jnp.dot(normed, wq[...], preferred_element_type=F32)
    for h in range(HEADS):
        b_q[h] = tiles(with_rows(q_part[:, h * 128 : (h + 1) * 128], sq_high, sq_low))
    for h in range(HEADS):
        owner = head_owner(h)
        slot = (kv - owner + N_KV) % N_KV

        @pl.when(owner != kv)
        def _():
            copy_to(b_q.at[h], r_q.at[slot], 1, (owner, tp)).start()

    ld_wk.wait()
    ld_wv.wait()
    k_part = jnp.dot(normed, wk[...], preferred_element_type=F32)
    v_part = jnp.dot(normed, wv[...], preferred_element_type=F32)
    for h in range(HEADS):
        b_kv[h, 0:3] = tiles(k_part[:, h * 128 : (h + 1) * 128])
        b_kv[h, 3:6] = tiles(v_part[:, h * 128 : (h + 1) * 128])
    for h in range(HEADS):
        owner = head_owner(h)
        slot = (kv - owner + N_KV) % N_KV

        @pl.when(owner != kv)
        def _():
            copy_to(b_kv.at[h], r_kv.at[slot], 2, (owner, tp)).start()

    @pl.when(is_head_owner)
    def _():
        wait_bytes(r_q.at[pl.ds(1, N_KV - 1)], recv_sem.at[1])
        total = up(b_q[own_head])
        for i in range(1, N_KV):
            total = total + up(r_q[i])
        square = total[SEQS : SEQS + 1] + total[SEQS + 1 : SEQS + 2]
        scale = row_to_column(lax.rsqrt(square / D + EPS))
        m_s[0, 0] = jnp.broadcast_to(scale, (ROWS, 128))
        q_all[own_head] = tiles(scale * total)
        for i in range(1, N_KV):
            copy_to(q_all.at[own_head], q_all.at[own_head], 3, (kv_peer(i), tp)).start()
        wait_bytes(q_all.at[pl.ds(0, HEADS - 1)], recv_sem.at[3])

    @pl.when(jnp.logical_not(is_head_owner))
    def _():
        wait_bytes(q_all, recv_sem.at[3])

    lane = iota((ROWS, 128), 1)
    for h in range(HEADS):
        q_h = up(q_all[h]) * 0.125
        q_s[pl.ds((2 * h) * ROWS, ROWS), :] = jnp.where(lane < 64, q_h, 0.0)
        q_s[pl.ds((2 * h + 1) * ROWS, ROWS), :] = jnp.where(lane >= 64, q_h, 0.0)
    ld_keys.wait()
    for s in range(SEQS):
        q_8 = q_s[pl.ds(s, 8, stride=ROWS), :].astype(BF16)
        part = lax.dot_general(
            q_8, keys[s], (((1,), (1,)), ((), ())), preferred_element_type=F32
        )
        for c in range(8):
            sc[c, pl.ds(s, 8, stride=ROWS), :] = part[:, c * 128 : (c + 1) * 128]

    for b in range(2 * HEADS):
        rows = pl.ds(b * ROWS, ROWS)
        mine = (iota((ROWS, 128), 1) % HEADS) == (b // 2)
        top = sc[0, rows, :]
        for c in range(1, 8):
            top = jnp.maximum(top, sc[c, rows, :])
        top = jnp.max(jnp.where(mine, top, LOW), axis=1, keepdims=True)
        total = jnp.zeros((ROWS, 128), F32)
        for c in range(8):
            weight = jnp.where(mine, jnp.exp(jnp.where(mine, sc[c, rows, :], LOW) - top), 0.0)
            sc[c, rows, :] = weight
            total = total + weight
        total = jnp.sum(total, axis=1, keepdims=True)
        m_s[1 + b // 2, b % 2] = jnp.broadcast_to(top, (ROWS, 128))
        l_s[1 + b // 2, b % 2] = jnp.broadcast_to(total, (ROWS, 128))

    ld_vals.wait()
    for s in range(SEQS):
        w_8 = jnp.concatenate(
            [sc[c, pl.ds(s, 8, stride=ROWS), :] for c in range(8)], axis=1
        ).astype(BF16)
        o_s[pl.ds(s, 8, stride=ROWS), :] = jnp.dot(w_8, vals[s], preferred_element_type=F32)

    def stat_row(col_b):
        shape = (ROWS, 128)
        row = jnp.sum(jnp.where(iota(shape, 0) == iota(shape, 1), col_b, 0.0), axis=0, keepdims=True)
        high = row.astype(BF16).astype(F32)
        mid = (row - high).astype(BF16).astype(F32)
        low = (row - high - mid).astype(BF16).astype(F32)
        at = iota((8, 128), 1)
        high, mid, low = (jnp.broadcast_to(v, (8, 128)) for v in (high, mid, low))
        packed = jnp.where(
            at < 32, high, jnp.where(at < 64, pltpu.roll(mid, 32, 1), pltpu.roll(low, 64, 1))
        )
        return packed[0:1]

    for b in range(2 * HEADS):
        h, mp = b // 2, b % 2
        block = with_rows(
            o_s[pl.ds(b * ROWS, ROWS), :], stat_row(m_s[1 + h, mp]), stat_row(l_s[1 + h, mp])
        )
        b_o[h, 3 * mp : 3 * mp + 3] = tiles(block)
    for h in range(HEADS):
        owner = head_owner(h)
        slot = (kv - owner + N_KV) % N_KV

        @pl.when(owner != kv)
        def _():
            copy_to(b_o.at[h], r_o.at[slot], 4, (owner, tp)).start()

    @pl.when(is_head_owner)
    def _():
        scale = m_s[0, 0]
        wait_bytes(r_kv.at[pl.ds(1, N_KV - 1)], recv_sem.at[2])
        k_sum = up(b_kv[own_head, 0:3])
        v_sum = up(b_kv[own_head, 3:6])
        for i in range(1, N_KV):
            k_sum = k_sum + up(r_kv[i, 0:3])
            v_sum = v_sum + up(r_kv[i, 3:6])
        k_new = (scale * k_sum).astype(BF16).astype(F32)
        v_new = (scale * v_sum).astype(BF16).astype(F32)
        product = up(q_all[own_head]) * k_new
        wait_bytes(r_o.at[pl.ds(1, N_KV - 1)], recv_sem.at[4])
        r_o[0] = b_o[own_head]
        pieces = iota((ROWS, 128), 1) % 32 == iota((ROWS, 128), 0)
        pieces = jnp.logical_and(pieces, iota((ROWS, 128), 1) < 96)

        def stat_col(row):
            spread = jnp.where(pieces, jnp.broadcast_to(row, (ROWS, 128)), 0.0)
            return jnp.broadcast_to(jnp.sum(spread, axis=1, keepdims=True), (ROWS, 128))

        results = []
        for mp in range(2):
            half = jnp.where((lane < 64) == (mp == 0), product, 0.0)
            new = jnp.sum(half, axis=1, keepdims=True) * 0.125
            peak = jnp.broadcast_to(new, (ROWS, 128))
            for i in range(N_KV):
                tile = r_o[i, 3 * mp + 2].astype(F32)
                m_i = stat_col(tile[6:7])
                l_s[i, mp] = stat_col(tile[7:8])
                m_s[i, mp] = m_i
                peak = jnp.maximum(peak, m_i)
            weight = jnp.exp(jnp.broadcast_to(new, (ROWS, 128)) - peak)
            numer = weight * v_new
            denom = weight
            for i in range(N_KV):
                weight = jnp.exp(m_s[i, mp] - peak)
                numer = numer + weight * up(r_o[i, 3 * mp : 3 * mp + 3])
                denom = denom + weight * l_s[i, mp]
            results.append(numer / denom)
        ld_lam.wait()
        ld_hgain.wait()
        mine = iota((1, HEADS), 1) == own_head
        lam_h = jnp.sum(jnp.where(mine, lam[...], 0.0), axis=1, keepdims=True)
        difference = results[0] - lam_h * results[1]
        mean = jnp.mean(difference * difference, axis=1, keepdims=True)
        h_all[own_head] = tiles(difference * lax.rsqrt(mean + EPS) * hgain[...])
        for i in range(1, N_KV):
            copy_to(h_all.at[own_head], h_all.at[own_head], 5, (kv_peer(i), tp)).start()
        wait_bytes(h_all.at[pl.ds(0, HEADS - 1)], recv_sem.at[5])

    @pl.when(jnp.logical_not(is_head_owner))
    def _():
        ld_lam.wait()
        ld_hgain.wait()
        wait_bytes(h_all, recv_sem.at[5])

    ld_wo.wait()
    heads_out = jnp.concatenate([up(h_all[h]) for h in range(HEADS)], axis=1).astype(BF16)
    r_b[tp] = tiles(jnp.dot(heads_out, wo[...], preferred_element_type=F32))
    for i in range(1, N_TP):
        copy_to(r_b.at[tp], r_b.at[tp], 6, (kv, tp_peer(i))).start()
    ld_mgain.wait()
    ld_wg.wait()
    ld_wu.wait()
    wait_bytes(r_b.at[pl.ds(0, N_TP - 1)], recv_sem.at[6])
    branch = up(r_b[0])
    for i in range(1, N_TP):
        branch = branch + up(r_b[i])
    live = iota((ROWS, 128), 0) < SEQS
    residual = jnp.where(live, (x_rows[...] + branch).astype(BF16).astype(F32), 0.0)
    normed_mid = (residual * mgain[...]).astype(BF16)
    sq_high, sq_low = split_two(
        column_to_row(jnp.sum(residual * residual, axis=1, keepdims=True))
    )

    across = (((1,), (1,)), ((), ()))
    gate_part = lax.dot_general(normed_mid, wg[...], across, preferred_element_type=F32)
    up_part = lax.dot_general(normed_mid, wu[...], across, preferred_element_type=F32)
    width = gate_part.shape[1]
    for j in range(CHUNKS):
        lo, hi = j * 128, min(j * 128 + 128, width)
        n = hi - lo
        at = iota((ROWS, n), 0)
        g_j = jnp.where(
            at == SEQS, sq_high[:, :n], jnp.where(at == SEQS + 1, sq_low[:, :n], gate_part[:, lo:hi])
        )
        u_j = up_part[:, lo:hi]
        b_g[j, 0:3, :, 0:n] = g_j.reshape(3, 8, n).astype(BF16)
        b_g[j, 3:6, :, 0:n] = u_j.reshape(3, 8, n).astype(BF16)

    def chunk_owner(j):
        return (32 * j) // CHUNKS + core

    k_chunk = kv - core
    own_chunk = jnp.clip((CHUNKS * k_chunk + 31) // 32, 0, CHUNKS - 1)
    is_chunk_owner = chunk_owner(own_chunk) == kv
    for j in range(CHUNKS):
        owner = chunk_owner(j)
        slot = (kv - owner + N_KV) % N_KV

        @pl.when(owner != kv)
        def _():
            copy_to(b_g.at[j], r_g.at[slot], 7, (owner, tp)).start()

    res_t[...] = jnp.transpose(
        jnp.concatenate([residual, jnp.zeros((128 - ROWS, 128), F32)], axis=0)
    ).reshape(N_TP, 16, 128)

    @pl.when(is_chunk_owner)
    def _():
        wait_bytes(r_g.at[pl.ds(1, N_KV - 1)], recv_sem.at[7])
        gate = up(b_g[own_chunk, 0:3])
        upper = up(b_g[own_chunk, 3:6])
        for i in range(1, N_KV):
            gate = gate + up(r_g[i, 0:3])
            upper = upper + up(r_g[i, 3:6])
        square = gate[SEQS : SEQS + 1] + gate[SEQS + 1 : SEQS + 2]
        scale = row_to_column(lax.rsqrt(square / D + EPS))
        gate = scale * gate
        hidden = (gate / (1.0 + jnp.exp(-gate))) * (scale * upper)
        hid[own_chunk] = tiles(hidden)
        for i in range(1, N_KV):
            copy_to(hid.at[own_chunk], hid.at[own_chunk], 8, (kv_peer(i), tp)).start()
        wait_bytes(hid.at[pl.ds(0, CHUNKS - 1)], recv_sem.at[8])

    @pl.when(jnp.logical_not(is_chunk_owner))
    def _():
        wait_bytes(hid, recv_sem.at[8])

    ld_wd.wait()
    hidden_all = jnp.concatenate([up(hid[j]) for j in range(CHUNKS)], axis=1).astype(BF16)
    down = jnp.dot(hidden_all, wd[...], preferred_element_type=F32)
    down_t = jnp.transpose(
        jnp.concatenate([down, jnp.zeros((128 - ROWS, 128), F32)], axis=0)
    )
    b_d[...] = down_t.reshape(N_TP, 16, 128).astype(BF16)
    r_d[tp] = b_d[tp]
    for i in range(1, N_TP):
        peer = tp_peer(i)
        copy_to(b_d.at[peer], r_d.at[tp], 9, (kv, peer)).start()
    wait_bytes(r_d.at[pl.ds(0, N_TP - 1)], recv_sem.at[9])
    mixer = r_d[0].astype(F32)
    for i in range(1, N_TP):
        mixer = mixer + r_d[i].astype(F32)
    out_ref[...] = (res_t[tp] + mixer).astype(BF16)[:, :SEQS]

    wait_bytes(x_all.at[pl.ds(0, N_TP - 1)], send_sem.at[0])
    wait_bytes(r_b.at[pl.ds(0, N_TP - 1)], send_sem.at[6])
    wait_bytes(r_d.at[pl.ds(0, N_TP - 1)], send_sem.at[9])

    @pl.when(is_head_owner)
    def _():
        wait_bytes(r_q.at[pl.ds(0, HEADS - 1)], send_sem.at[1])
        wait_bytes(r_kv.at[pl.ds(0, HEADS - 1)], send_sem.at[2])
        wait_bytes(r_q.at[pl.ds(1, N_KV - 1)], send_sem.at[3])
        wait_bytes(r_o.at[pl.ds(0, HEADS - 1)], send_sem.at[4])
        wait_bytes(r_q.at[pl.ds(1, N_KV - 1)], send_sem.at[5])

    @pl.when(jnp.logical_not(is_head_owner))
    def _():
        wait_bytes(r_q.at[pl.ds(0, HEADS)], send_sem.at[1])
        wait_bytes(r_kv.at[pl.ds(0, HEADS)], send_sem.at[2])
        wait_bytes(r_o.at[pl.ds(0, HEADS)], send_sem.at[4])

    @pl.when(is_chunk_owner)
    def _():
        wait_bytes(r_g.at[pl.ds(0, CHUNKS - 1)], send_sem.at[7])
        wait_bytes(r_q.at[pl.ds(1, N_KV - 1)], send_sem.at[8])

    @pl.when(jnp.logical_not(is_chunk_owner))
    def _():
        wait_bytes(r_g.at[pl.ds(0, CHUNKS)], send_sem.at[7])


def per_device(
    tokens, attn_gain, w_query, w_key, w_value, cache_keys, cache_values, lambdas, head_gain,
    w_out, mlp_gain, w_gate, w_up, w_down,
):
    seqs, positions, heads, dim = cache_keys.shape
    args = (
        tokens.T, attn_gain.reshape(1, -1), w_query, w_key, w_value,
        cache_keys.reshape(seqs, positions * heads, dim),
        cache_values.reshape(seqs, positions * heads, dim),
        lambdas.reshape(1, -1), head_gain.reshape(1, -1), w_out, mlp_gain.reshape(1, -1),
        w_gate.T, w_up.T, w_down,
    )
    vmem = pltpu.VMEM
    local = [vmem(a.shape, a.dtype) for a in args]
    local[-1] = vmem((CHUNKS * 128, 128), BF16)
    tile = (3, 8, 128)
    pair = (6, 8, 128)
    scratch = local + [
        vmem((N_TP, 16, 128), BF16),
        vmem((ROWS, 128), F32),
        vmem((HEADS, *tile), BF16),
        vmem((N_KV, *tile), BF16),
        vmem((HEADS, *pair), BF16),
        vmem((N_KV, *pair), BF16),
        vmem((HEADS, *tile), BF16),
        vmem((2 * HEADS * ROWS, 128), F32),
        vmem((8, 2 * HEADS * ROWS, 128), F32),
        vmem((2 * HEADS * ROWS, 128), F32),
        vmem((HEADS, *pair), BF16),
        vmem((N_KV, *pair), BF16),
        vmem((N_KV, 2, ROWS, 128), F32),
        vmem((N_KV, 2, ROWS, 128), F32),
        vmem((HEADS, *tile), BF16),
        vmem((N_TP, *tile), BF16),
        vmem((N_TP, 16, 128), F32),
        vmem((CHUNKS, *pair), BF16),
        vmem((N_KV, *pair), BF16),
        vmem((CHUNKS, *tile), BF16),
        vmem((N_TP, 16, 128), BF16),
        vmem((N_TP, 16, 128), BF16),
        pltpu.SemaphoreType.DMA((len(args),)),
        pltpu.SemaphoreType.DMA((10,)),
        pltpu.SemaphoreType.DMA((10,)),
    ]
    out = pl.pallas_call(
        kernel,
        out_shape=jax.ShapeDtypeStruct((tokens.shape[1], seqs), BF16),
        in_specs=[pl.BlockSpec(memory_space=pl.ANY)] * len(args),
        out_specs=pl.BlockSpec(memory_space=pltpu.VMEM),
        scratch_shapes=scratch,
        compiler_params=pltpu.CompilerParams(
            collective_id=0, has_side_effects=True, vmem_limit_bytes=60 * 1024 * 1024
        ),
        name="decode_step",
    )(*args)
    return out.T


def solution(mesh):
    placed = (
        P(None, ("kv", "tp")), P("kv"), P("kv", "tp"), P("kv", "tp"), P("kv", "tp"),
        P(None, "kv", "tp", None), P(None, "kv", "tp", None), P("tp"), P(), P("tp", "kv"),
        P("kv"), P("kv", "tp"), P("kv", "tp"), P("tp", "kv"),
    )
    return jax.shard_map(
        per_device, mesh=mesh, in_specs=placed, out_specs=P(None, ("kv", "tp")), check_vma=False
    )
```

time: 191 us -> 67.9 us (0.36)
  blocking collectives: 80.4 us -> 0 us
  Pallas kernels: 0 us -> 66.5 us
  waiting for transfers between devices: 34.3 us -> 0 us
  starting transfers between devices: 27 us -> 0 us
  local copies, waits for them, and re-layouts: 24.4 us -> 1.28 us
  matrix products: 19.7 us -> 0 us
  other arithmetic: 3.54 us -> 0 us
    pallas_call x0 -> x1, Pallas kernels: none -> 66.5 us  [per_device(): pl.pallas_call(kernel, out_shape=jax.ShapeDtypeStruct((tokens.shape[1], s...]
    all_to_all x3 -> x0, blocking collectives: 48.5 us -> none  [the longest x2 28.2 us: from_everyone(): return lax.all_to_all(copies, axis, split_axis=0, concat_axis=0, tiled=True)]
    all_to_all x5 -> x0, waiting for transfers between devices: 34.3 us -> none  [the longest x3 18.8 us: from_everyone(): return lax.all_to_all(copies, axis, split_axis=0, concat_axis=0, tiled=True)]
    all_gather x2 -> x0, blocking collectives: 31.9 us -> none  [all_in_one(): both, at, found = (lax.all_gather(jnp.concatenate(lines), axis), 0, {})]
    all_to_all x5 -> x0, starting transfers between devices: 27 us -> none  [the longest x3 12.4 us: from_everyone(): return lax.all_to_all(copies, axis, split_axis=0, concat_axis=0, tiled=True)]
    dot_general x11 -> x0, matrix products: 19.7 us -> none  [the longest x2 8.45 us: partial_map(): jnp.einsum('shd,sthd->sht', query_rows[:, :, low:high], cache_keys[:, :,...]
    slice x9 -> x0, local copies, waits for them, and re-layouts: 13 us -> none  [the longest x1 12.1 us: partial_map(): cache_keys[:, :, :, low:high]]
    broadcast_in_dim x4 -> x0, local copies, waits for them, and re-layouts: 2.15 us -> none  [from_everyone(): copies = jnp.broadcast_to(shard, (lax.axis_size(axis), *shard.shape))]
  transfers between devices with their start and end apart: 5 -> 0, of which waited for: 4 -> 0; matrix products, arithmetic and copies ran while one was open for 7% -> 0% of each run, Pallas kernels for 0% -> 0%
where the time goes in v1:
time: 67.9 us; the launch traced here: 67.8 us
  Pallas kernels  66.5 us (98%)
  local copies, waits for them, and re-layouts  1.28 us (2%)
    pallas_call x1, Pallas kernels, per_device(): pl.pallas_call(kernel, out_shape=jax.ShapeDtypeStruct((tokens.shape[1], s...  66.5 us

profile of v1, /device:TPU:1, one launch (start us, length us, event | category | flops | bytes accessed | tf_op | source)
XLA Modules:
  0.0 67.8 jit_solution(15876765430874094631)
XLA Ops:
  0.0 66.5 %decode_step.1 = bf16[16,22]{1,0:T(8,128)(2,1)} custom-call(bf16[16,22]{1,0:T(8,128)(2,1)} %bitcast.15, f32[1,128]{1,0:T(1,128)} %bitcast.16, bf16[128,512]{1,0:T(8,128)(2,1)} %wq_hbm.1, bf16[128,512]{1,0:T(8,128)(2,1)} %wk_hbm.1, bf16[128,512]{1,0:T(8,128)(2,1)} %wv_hbm.1, bf16[22,1024,128]{2,1,0:T(8,128)(2,1)} %bitcast.10, ...), custom_call_target="tpu_custom_call" | custom-call | tf_op jit(solution)/shard_map/decode_step/pallas_call | solution.py:470
  66.5 1.3 %copy.16 = bf16[22,16]{0,1:T(8,128)(2,1)} copy(bf16[22,16]{0,1:T(8,128)(2,1)} %bitcast.14) | data formatting | bytes 1408

commit v2 on v1

--- a/solution.py
+++ b/solution.py
@@ -14,9 +14,19 @@
 ROWS = 24
 SEQS = 22
 N_KV, N_X, N_TP = 32, 4, 8
+N_Z = N_KV // N_X
+KV_ORDER = sorted(
+    range(1, N_KV),
+    key=lambda i: -(min(i // N_X, N_Z - i // N_X) + min(i % N_X, N_X - i % N_X)),
+)
+TP_ORDER = (4, 5, 3, 2, 6, 7, 1)
+PLANES = sorted(range(N_Z), key=lambda p: min(p, N_Z - p))
 HEADS = 4
 CHUNKS = 11
 LOW = -3.0e38
+QUERY_OWNERS = ((0, 8, 16, 24), (6, 14, 22, 30))
+HEAD_OWNERS = ((0, 6, 8, 14), (1, 7, 9, 15))
+CHUNK_OWNERS = ((0, 2, 5, 8, 11, 14, 17, 20, 23, 26, 29), (1, 3, 6, 9, 12, 15, 18, 21, 24, 27, 30))
 
 
 def up(block):
@@ -61,7 +71,7 @@
     x_all, x_rows,
     b_q, r_q, b_kv, r_kv, q_all, q_s, sc, o_s,
     b_o, r_o, m_s, l_s, h_all, r_b, res_t, b_g, r_g, hid, b_d, r_d,
-    load_sem, send_sem, recv_sem,
+    keys_t, load_sem, send_sem, recv_sem,
 ):
     kv = lax.axis_index("kv")
     tp = lax.axis_index("tp")
@@ -69,17 +79,36 @@
     x = kv % N_X
     core = tp % 2
 
+    def kv_slot(owner):
+        return ((z - owner // N_X) % N_Z) * N_X + (x - owner % N_X) % N_X
+
     def kv_peer(i):
-        return ((z + i // N_X) % (N_KV // N_X)) * N_X + (x + i % N_X) % N_X
+        return ((z + i // N_X) % N_Z) * N_X + (x + i % N_X) % N_X
 
     def tp_peer(i):
         return (tp + i) % N_TP
+
+    def owner_in(table, n):
+        return table[0][n] + (table[1][n] - table[0][n]) * core
+
+    def own_in(table):
+        at = [(kv == owner_in(table, n)).astype(jnp.int32) for n in range(len(table[0]))]
+        return sum(n * hit for n, hit in enumerate(at)), sum(at) > 0
+
+    query_head, is_query_owner = own_in(QUERY_OWNERS)
+    own_head, is_head_owner = own_in(HEAD_OWNERS)
+    own_chunk, is_chunk_owner = own_in(CHUNK_OWNERS)
 
     barrier = pltpu.get_barrier_semaphore()
     for i in range(1, N_TP):
         pl.semaphore_signal(barrier, inc=1, device_id=(kv, tp_peer(i)), device_id_type=MESH)
-    for i in range(1, N_KV):
-        pl.semaphore_signal(barrier, inc=1, device_id=(kv_peer(i), tp), device_id_type=MESH)
+
+    for role in (is_query_owner, is_head_owner):
+
+        @pl.when(role)
+        def _():
+            for i in KV_ORDER:
+                pl.semaphore_signal(barrier, inc=1, device_id=(kv_peer(i), tp), device_id_type=MESH)
 
     loads = [
         pltpu.make_async_copy(src, dst, load_sem.at[n])
@@ -97,11 +126,17 @@
     (ld_tok, ld_again, ld_wq, ld_wk, ld_wv, ld_keys, ld_vals, ld_lam, ld_hgain, ld_wo, ld_mgain,
      ld_wg, ld_wu, ld_wd) = loads
 
-    def copy_to(src, dst, phase, device):
+    def copy_to(src, dst, phase, device, plane=0):
         return pltpu.make_async_remote_copy(
-            src_ref=src, dst_ref=dst, send_sem=send_sem.at[phase], recv_sem=recv_sem.at[phase],
-            device_id=device, device_id_type=MESH,
+            src_ref=src, dst_ref=dst, send_sem=send_sem.at[phase],
+            recv_sem=recv_sem.at[phase, plane], device_id=device, device_id_type=MESH,
         )
+
+    def plane_slots(ref, phase, p):
+        first = 1 if p == 0 else p * N_X
+        count = p * N_X + N_X - first
+        wait_bytes(ref.at[pl.ds(first, count)], recv_sem.at[phase, p])
+        return range(first, first + count)
 
     def wait_bytes(ref, sem):
         pltpu.make_async_copy(ref, ref, sem).wait()
@@ -119,13 +154,14 @@
     x_all[tp] = jnp.concatenate(
         [tok_v[...].astype(F32), jnp.zeros((16, 128 - SEQS), F32)], axis=1
     ).astype(BF16)
-    pl.semaphore_wait(barrier, N_TP - 1 + N_KV - 1)
-
-    for i in range(1, N_TP):
+    own_roles = is_query_owner.astype(jnp.int32) + is_head_owner.astype(jnp.int32)
+    pl.semaphore_wait(barrier, N_TP - 1 + 2 * HEADS - own_roles)
+
+    for i in TP_ORDER:
         copy_to(x_all.at[tp], x_all.at[tp], 0, (kv, tp_peer(i))).start()
     ld_again.wait()
     ld_wq.wait()
-    wait_bytes(x_all.at[pl.ds(0, N_TP - 1)], recv_sem.at[0])
+    wait_bytes(x_all.at[pl.ds(0, N_TP - 1)], recv_sem.at[0, 0])
     x_cols = x_all[...].astype(F32).reshape(128, 128)
     x_f = jnp.transpose(x_cols)[:ROWS]
     x_rows[...] = x_f
@@ -133,68 +169,66 @@
     square_row = column_to_row(jnp.sum(x_f * x_f, axis=1, keepdims=True))
     sq_high, sq_low = split_two(square_row)
 
-    def head_owner(h):
-        return 8 * h + 6 * core
-
-    k_own = kv - 6 * core
-    own_head = jnp.clip(k_own // 8, 0, HEADS - 1)
-    is_head_owner = (kv == head_owner(own_head))
-
     q_part = jnp.dot(normed, wq[...], preferred_element_type=F32)
     for h in range(HEADS):
         b_q[h] = tiles(with_rows(q_part[:, h * 128 : (h + 1) * 128], sq_high, sq_low))
     for h in range(HEADS):
-        owner = head_owner(h)
-        slot = (kv - owner + N_KV) % N_KV
+        owner = owner_in(QUERY_OWNERS, h)
+        slot = kv_slot(owner)
 
         @pl.when(owner != kv)
         def _():
-            copy_to(b_q.at[h], r_q.at[slot], 1, (owner, tp)).start()
+            copy_to(b_q.at[h], r_q.at[slot], 1, (owner, tp), slot // N_X).start()
 
     ld_wk.wait()
     ld_wv.wait()
     k_part = jnp.dot(normed, wk[...], preferred_element_type=F32)
     v_part = jnp.dot(normed, wv[...], preferred_element_type=F32)
     for h in range(HEADS):
-        b_kv[h, 0:3] = tiles(k_part[:, h * 128 : (h + 1) * 128])
+        b_kv[h, 0:3] = tiles(with_rows(k_part[:, h * 128 : (h + 1) * 128], sq_high, sq_low))
         b_kv[h, 3:6] = tiles(v_part[:, h * 128 : (h + 1) * 128])
     for h in range(HEADS):
-        owner = head_owner(h)
-        slot = (kv - owner + N_KV) % N_KV
+        owner = owner_in(HEAD_OWNERS, h)
+        slot = kv_slot(owner)
 
         @pl.when(owner != kv)
         def _():
-            copy_to(b_kv.at[h], r_kv.at[slot], 2, (owner, tp)).start()
-
-    @pl.when(is_head_owner)
-    def _():
-        wait_bytes(r_q.at[pl.ds(1, N_KV - 1)], recv_sem.at[1])
-        total = up(b_q[own_head])
-        for i in range(1, N_KV):
-            total = total + up(r_q[i])
+            copy_to(b_kv.at[h], r_kv.at[slot], 2, (owner, tp), slot // N_X).start()
+
+    @pl.when(is_query_owner)
+    def _():
+        total = up(b_q[query_head])
+        for p in PLANES:
+            for i in plane_slots(r_q, 1, p):
+                total = total + up(r_q[i])
         square = total[SEQS : SEQS + 1] + total[SEQS + 1 : SEQS + 2]
         scale = row_to_column(lax.rsqrt(square / D + EPS))
-        m_s[0, 0] = jnp.broadcast_to(scale, (ROWS, 128))
-        q_all[own_head] = tiles(scale * total)
-        for i in range(1, N_KV):
-            copy_to(q_all.at[own_head], q_all.at[own_head], 3, (kv_peer(i), tp)).start()
-        wait_bytes(q_all.at[pl.ds(0, HEADS - 1)], recv_sem.at[3])
-
-    @pl.when(jnp.logical_not(is_head_owner))
-    def _():
-        wait_bytes(q_all, recv_sem.at[3])
+        q_all[query_head] = tiles(scale * total)
+        for i in KV_ORDER:
+            copy_to(q_all.at[query_head], q_all.at[query_head], 3, (kv_peer(i), tp)).start()
+
+    ld_keys.wait()
+    for s in range(SEQS):
+        keys_t[s] = jnp.transpose(keys[s])
+
+    role = is_query_owner
+
+    @pl.when(role)
+    def _():
+        wait_bytes(q_all.at[pl.ds(0, HEADS - 1)], recv_sem.at[3, 0])
+
+    @pl.when(jnp.logical_not(role))
+    def _():
+        wait_bytes(q_all, recv_sem.at[3, 0])
 
     lane = iota((ROWS, 128), 1)
     for h in range(HEADS):
         q_h = up(q_all[h]) * 0.125
         q_s[pl.ds((2 * h) * ROWS, ROWS), :] = jnp.where(lane < 64, q_h, 0.0)
         q_s[pl.ds((2 * h + 1) * ROWS, ROWS), :] = jnp.where(lane >= 64, q_h, 0.0)
-    ld_keys.wait()
     for s in range(SEQS):
         q_8 = q_s[pl.ds(s, 8, stride=ROWS), :].astype(BF16)
-        part = lax.dot_general(
-            q_8, keys[s], (((1,), (1,)), ((), ())), preferred_element_type=F32
-        )
+        part = jnp.dot(q_8, keys_t[s], preferred_element_type=F32)
         for c in range(8):
             sc[c, pl.ds(s, 8, stride=ROWS), :] = part[:, c * 128 : (c + 1) * 128]
 
@@ -241,26 +275,26 @@
         )
         b_o[h, 3 * mp : 3 * mp + 3] = tiles(block)
     for h in range(HEADS):
-        owner = head_owner(h)
-        slot = (kv - owner + N_KV) % N_KV
+        owner = owner_in(HEAD_OWNERS, h)
+        slot = kv_slot(owner)
 
         @pl.when(owner != kv)
         def _():
-            copy_to(b_o.at[h], r_o.at[slot], 4, (owner, tp)).start()
+            copy_to(b_o.at[h], r_o.at[slot], 4, (owner, tp), slot // N_X).start()
 
     @pl.when(is_head_owner)
     def _():
-        scale = m_s[0, 0]
-        wait_bytes(r_kv.at[pl.ds(1, N_KV - 1)], recv_sem.at[2])
         k_sum = up(b_kv[own_head, 0:3])
         v_sum = up(b_kv[own_head, 3:6])
-        for i in range(1, N_KV):
-            k_sum = k_sum + up(r_kv[i, 0:3])
-            v_sum = v_sum + up(r_kv[i, 3:6])
+        for p in PLANES:
+            for i in plane_slots(r_kv, 2, p):
+                k_sum = k_sum + up(r_kv[i, 0:3])
+                v_sum = v_sum + up(r_kv[i, 3:6])
+        square = k_sum[SEQS : SEQS + 1] + k_sum[SEQS + 1 : SEQS + 2]
+        scale = row_to_column(lax.rsqrt(square / D + EPS))
         k_new = (scale * k_sum).astype(BF16).astype(F32)
         v_new = (scale * v_sum).astype(BF16).astype(F32)
         product = up(q_all[own_head]) * k_new
-        wait_bytes(r_o.at[pl.ds(1, N_KV - 1)], recv_sem.at[4])
         r_o[0] = b_o[own_head]
         pieces = iota((ROWS, 128), 1) % 32 == iota((ROWS, 128), 0)
         pieces = jnp.logical_and(pieces, iota((ROWS, 128), 1) < 96)
@@ -269,25 +303,30 @@
             spread = jnp.where(pieces, jnp.broadcast_to(row, (ROWS, 128)), 0.0)
             return jnp.broadcast_to(jnp.sum(spread, axis=1, keepdims=True), (ROWS, 128))
 
-        results = []
+        peak, denom, numer = [], [], []
         for mp in range(2):
             half = jnp.where((lane < 64) == (mp == 0), product, 0.0)
             new = jnp.sum(half, axis=1, keepdims=True) * 0.125
-            peak = jnp.broadcast_to(new, (ROWS, 128))
-            for i in range(N_KV):
-                tile = r_o[i, 3 * mp + 2].astype(F32)
-                m_i = stat_col(tile[6:7])
-                l_s[i, mp] = stat_col(tile[7:8])
-                m_s[i, mp] = m_i
-                peak = jnp.maximum(peak, m_i)
-            weight = jnp.exp(jnp.broadcast_to(new, (ROWS, 128)) - peak)
-            numer = weight * v_new
-            denom = weight
-            for i in range(N_KV):
-                weight = jnp.exp(m_s[i, mp] - peak)
-                numer = numer + weight * up(r_o[i, 3 * mp : 3 * mp + 3])
-                denom = denom + weight * l_s[i, mp]
-            results.append(numer / denom)
+            peak.append(jnp.broadcast_to(new, (ROWS, 128)))
+            denom.append(jnp.ones((ROWS, 128), F32))
+            numer.append(v_new)
+        for p in PLANES:
+            slots = list(plane_slots(r_o, 4, p))
+            if p == 0:
+                slots.append(0)
+            for mp in range(2):
+                last = [r_o[i, 3 * mp + 2].astype(F32) for i in slots]
+                tops = [stat_col(tile[6:7]) for tile in last]
+                totals = [stat_col(tile[7:8]) for tile in last]
+                above = functools.reduce(jnp.maximum, tops, peak[mp])
+                fade = jnp.exp(peak[mp] - above)
+                n, d = numer[mp] * fade, denom[mp] * fade
+                for i, top, total in zip(slots, tops, totals):
+                    weight = jnp.exp(top - above)
+                    n = n + weight * up(r_o[i, 3 * mp : 3 * mp + 3])
+                    d = d + weight * total
+                peak[mp], numer[mp], denom[mp] = above, n, d
+        results = [numer[mp] / denom[mp] for mp in range(2)]
         ld_lam.wait()
         ld_hgain.wait()
         mine = iota((1, HEADS), 1) == own_head
@@ -295,25 +334,25 @@
         difference = results[0] - lam_h * results[1]
         mean = jnp.mean(difference * difference, axis=1, keepdims=True)
         h_all[own_head] = tiles(difference * lax.rsqrt(mean + EPS) * hgain[...])
-        for i in range(1, N_KV):
+        for i in KV_ORDER:
             copy_to(h_all.at[own_head], h_all.at[own_head], 5, (kv_peer(i), tp)).start()
-        wait_bytes(h_all.at[pl.ds(0, HEADS - 1)], recv_sem.at[5])
+        wait_bytes(h_all.at[pl.ds(0, HEADS - 1)], recv_sem.at[5, 0])
 
     @pl.when(jnp.logical_not(is_head_owner))
     def _():
         ld_lam.wait()
         ld_hgain.wait()
-        wait_bytes(h_all, recv_sem.at[5])
+        wait_bytes(h_all, recv_sem.at[5, 0])
 
     ld_wo.wait()
     heads_out = jnp.concatenate([up(h_all[h]) for h in range(HEADS)], axis=1).astype(BF16)
     r_b[tp] = tiles(jnp.dot(heads_out, wo[...], preferred_element_type=F32))
-    for i in range(1, N_TP):
+    for i in TP_ORDER:
         copy_to(r_b.at[tp], r_b.at[tp], 6, (kv, tp_peer(i))).start()
     ld_mgain.wait()
     ld_wg.wait()
     ld_wu.wait()
-    wait_bytes(r_b.at[pl.ds(0, N_TP - 1)], recv_sem.at[6])
+    wait_bytes(r_b.at[pl.ds(0, N_TP - 1)], recv_sem.at[6, 0])
     branch = up(r_b[0])
     for i in range(1, N_TP):
         branch = branch + up(r_b[i])
@@ -325,33 +364,22 @@
     )
 
     across = (((1,), (1,)), ((), ()))
-    gate_part = lax.dot_general(normed_mid, wg[...], across, preferred_element_type=F32)
-    up_part = lax.dot_general(normed_mid, wu[...], across, preferred_element_type=F32)
-    width = gate_part.shape[1]
+    width = wg.shape[0]
     for j in range(CHUNKS):
         lo, hi = j * 128, min(j * 128 + 128, width)
         n = hi - lo
         at = iota((ROWS, n), 0)
-        g_j = jnp.where(
-            at == SEQS, sq_high[:, :n], jnp.where(at == SEQS + 1, sq_low[:, :n], gate_part[:, lo:hi])
-        )
-        u_j = up_part[:, lo:hi]
+        g_j = lax.dot_general(normed_mid, wg[lo:hi, :], across, preferred_element_type=F32)
+        u_j = lax.dot_general(normed_mid, wu[lo:hi, :], across, preferred_element_type=F32)
+        g_j = jnp.where(at == SEQS, sq_high[:, :n], jnp.where(at == SEQS + 1, sq_low[:, :n], g_j))
         b_g[j, 0:3, :, 0:n] = g_j.reshape(3, 8, n).astype(BF16)
         b_g[j, 3:6, :, 0:n] = u_j.reshape(3, 8, n).astype(BF16)
-
-    def chunk_owner(j):
-        return (32 * j) // CHUNKS + core
-
-    k_chunk = kv - core
-    own_chunk = jnp.clip((CHUNKS * k_chunk + 31) // 32, 0, CHUNKS - 1)
-    is_chunk_owner = chunk_owner(own_chunk) == kv
-    for j in range(CHUNKS):
-        owner = chunk_owner(j)
-        slot = (kv - owner + N_KV) % N_KV
+        owner = owner_in(CHUNK_OWNERS, j)
+        slot = kv_slot(owner)
 
         @pl.when(owner != kv)
         def _():
-            copy_to(b_g.at[j], r_g.at[slot], 7, (owner, tp)).start()
+            copy_to(b_g.at[j], r_g.at[slot], 7, (owner, tp), slot // N_X).start()
 
     res_t[...] = jnp.transpose(
         jnp.concatenate([residual, jnp.zeros((128 - ROWS, 128), F32)], axis=0)
@@ -359,24 +387,24 @@
 
     @pl.when(is_chunk_owner)
     def _():
-        wait_bytes(r_g.at[pl.ds(1, N_KV - 1)], recv_sem.at[7])
         gate = up(b_g[own_chunk, 0:3])
         upper = up(b_g[own_chunk, 3:6])
-        for i in range(1, N_KV):
-            gate = gate + up(r_g[i, 0:3])
-            upper = upper + up(r_g[i, 3:6])
+        for p in PLANES:
+            for i in plane_slots(r_g, 7, p):
+                gate = gate + up(r_g[i, 0:3])
+                upper = upper + up(r_g[i, 3:6])
         square = gate[SEQS : SEQS + 1] + gate[SEQS + 1 : SEQS + 2]
         scale = row_to_column(lax.rsqrt(square / D + EPS))
         gate = scale * gate
         hidden = (gate / (1.0 + jnp.exp(-gate))) * (scale * upper)
         hid[own_chunk] = tiles(hidden)
-        for i in range(1, N_KV):
+        for i in KV_ORDER:
             copy_to(hid.at[own_chunk], hid.at[own_chunk], 8, (kv_peer(i), tp)).start()
-        wait_bytes(hid.at[pl.ds(0, CHUNKS - 1)], recv_sem.at[8])
+        wait_bytes(hid.at[pl.ds(0, CHUNKS - 1)], recv_sem.at[8, 0])
 
     @pl.when(jnp.logical_not(is_chunk_owner))
     def _():
-        wait_bytes(hid, recv_sem.at[8])
+        wait_bytes(hid, recv_sem.at[8, 0])
 
     ld_wd.wait()
     hidden_all = jnp.concatenate([up(hid[j]) for j in range(CHUNKS)], axis=1).astype(BF16)
@@ -386,10 +414,10 @@
     )
     b_d[...] = down_t.reshape(N_TP, 16, 128).astype(BF16)
     r_d[tp] = b_d[tp]
-    for i in range(1, N_TP):
+    for i in TP_ORDER:
         peer = tp_peer(i)
         copy_to(b_d.at[peer], r_d.at[tp], 9, (kv, peer)).start()
-    wait_bytes(r_d.at[pl.ds(0, N_TP - 1)], recv_sem.at[9])
+    wait_bytes(r_d.at[pl.ds(0, N_TP - 1)], recv_sem.at[9, 0])
     mixer = r_d[0].astype(F32)
     for i in range(1, N_TP):
         mixer = mixer + r_d[i].astype(F32)
@@ -399,17 +427,23 @@
     wait_bytes(r_b.at[pl.ds(0, N_TP - 1)], send_sem.at[6])
     wait_bytes(r_d.at[pl.ds(0, N_TP - 1)], send_sem.at[9])
 
+    @pl.when(is_query_owner)
+    def _():
+        wait_bytes(r_q.at[pl.ds(0, HEADS - 1)], send_sem.at[1])
+        wait_bytes(r_q.at[pl.ds(1, N_KV - 1)], send_sem.at[3])
+
+    @pl.when(jnp.logical_not(is_query_owner))
+    def _():
+        wait_bytes(r_q.at[pl.ds(0, HEADS)], send_sem.at[1])
+
     @pl.when(is_head_owner)
     def _():
-        wait_bytes(r_q.at[pl.ds(0, HEADS - 1)], send_sem.at[1])
         wait_bytes(r_kv.at[pl.ds(0, HEADS - 1)], send_sem.at[2])
-        wait_bytes(r_q.at[pl.ds(1, N_KV - 1)], send_sem.at[3])
         wait_bytes(r_o.at[pl.ds(0, HEADS - 1)], send_sem.at[4])
         wait_bytes(r_q.at[pl.ds(1, N_KV - 1)], send_sem.at[5])
 
     @pl.when(jnp.logical_not(is_head_owner))
     def _():
-        wait_bytes(r_q.at[pl.ds(0, HEADS)], send_sem.at[1])
         wait_bytes(r_kv.at[pl.ds(0, HEADS)], send_sem.at[2])
         wait_bytes(r_o.at[pl.ds(0, HEADS)], send_sem.at[4])
 
@@ -463,13 +497,14 @@
         vmem((CHUNKS, *tile), BF16),
         vmem((N_TP, 16, 128), BF16),
         vmem((N_TP, 16, 128), BF16),
+        vmem((seqs, dim, positions * heads), BF16),
         pltpu.SemaphoreType.DMA((len(args),)),
         pltpu.SemaphoreType.DMA((10,)),
-        pltpu.SemaphoreType.DMA((10,)),
+        pltpu.SemaphoreType.DMA((10, N_Z)),
     ]
     out = pl.pallas_call(
         kernel,
-        out_shape=jax.ShapeDtypeStruct((tokens.shape[1], seqs), BF16),
+        out_shape=pltpu.VMEM((tokens.shape[1], seqs), BF16),
         in_specs=[pl.BlockSpec(memory_space=pl.ANY)] * len(args),
         out_specs=pl.BlockSpec(memory_space=pltpu.VMEM),
         scratch_shapes=scratch,

time: 67.9 us -> 61.9 us (0.912)
  Pallas kernels: 66.5 us -> 61.2 us
  local copies, waits for them, and re-layouts: 1.28 us -> 0.6 us
    pallas_call x1, Pallas kernels: 66.5 us -> 61.2 us  [per_device(): pl.pallas_call(kernel, out_shape=pltpu.VMEM((tokens.shape[1], seqs), BF16...]
    unnamed x1, local copies, waits for them, and re-layouts: 1.28 us -> 0.6 us
where the time goes in v2:
time: 61.9 us; the launch traced here: 61.8 us
  Pallas kernels  61.2 us (99%)
    pallas_call x1, Pallas kernels, per_device(): pl.pallas_call(kernel, out_shape=pltpu.VMEM((tokens.shape[1], seqs), BF16...  61.2 us

profile of v2, /device:TPU:1, one launch (start us, length us, event | category | flops | bytes accessed | tf_op | source)
XLA Modules:
  0.0 61.8 jit_solution(12531885964389286113)
XLA Ops:
  0.0 61.2 %decode_step.1 = bf16[16,22]{1,0:T(8,128)(2,1)S(1)} custom-call(bf16[16,22]{1,0:T(8,128)(2,1)} %bitcast.15, f32[1,128]{1,0:T(1,128)} %bitcast.16, bf16[128,512]{1,0:T(8,128)(2,1)} %wq_hbm.1, bf16[128,512]{1,0:T(8,128)(2,1)} %wk_hbm.1, bf16[128,512]{1,0:T(8,128)(2,1)} %wv_hbm.1, bf16[22,1024,128]{2,1,0:T(8,128)(2,1)} %bitcast.11, ...), custom_call_target="tpu_custom_call" | custom-call | tf_op jit(solution)/shard_map/decode_step/pallas_call | solution.py:505
  61.2 0.6 copy.16

commit v3 on v2

--- a/solution.py
+++ b/solution.py
@@ -71,7 +71,7 @@
     x_all, x_rows,
     b_q, r_q, b_kv, r_kv, q_all, q_s, sc, o_s,
     b_o, r_o, m_s, l_s, h_all, r_b, res_t, b_g, r_g, hid, b_d, r_d,
-    keys_t, load_sem, send_sem, recv_sem,
+    keys_t, wg_t, wu_t, load_sem, send_sem, recv_sem,
 ):
     kv = lax.axis_index("kv")
     tp = lax.axis_index("tp")
@@ -281,6 +281,9 @@
         @pl.when(owner != kv)
         def _():
             copy_to(b_o.at[h], r_o.at[slot], 4, (owner, tp), slot // N_X).start()
+
+    ld_lam.wait()
+    ld_hgain.wait()
 
     @pl.when(is_head_owner)
     def _():
@@ -327,8 +330,6 @@
                     d = d + weight * total
                 peak[mp], numer[mp], denom[mp] = above, n, d
         results = [numer[mp] / denom[mp] for mp in range(2)]
-        ld_lam.wait()
-        ld_hgain.wait()
         mine = iota((1, HEADS), 1) == own_head
         lam_h = jnp.sum(jnp.where(mine, lam[...], 0.0), axis=1, keepdims=True)
         difference = results[0] - lam_h * results[1]
@@ -336,12 +337,21 @@
         h_all[own_head] = tiles(difference * lax.rsqrt(mean + EPS) * hgain[...])
         for i in KV_ORDER:
             copy_to(h_all.at[own_head], h_all.at[own_head], 5, (kv_peer(i), tp)).start()
+
+    ld_wg.wait()
+    ld_wu.wait()
+    width = wg.shape[0]
+    for j in range(CHUNKS):
+        lo, hi = j * 128, min(j * 128 + 128, width)
+        wg_t[j, :, 0 : hi - lo] = jnp.transpose(wg[lo:hi, :])
+        wu_t[j, :, 0 : hi - lo] = jnp.transpose(wu[lo:hi, :])
+
+    @pl.when(is_head_owner)
+    def _():
         wait_bytes(h_all.at[pl.ds(0, HEADS - 1)], recv_sem.at[5, 0])
 
     @pl.when(jnp.logical_not(is_head_owner))
     def _():
-        ld_lam.wait()
-        ld_hgain.wait()
         wait_bytes(h_all, recv_sem.at[5, 0])
 
     ld_wo.wait()
@@ -350,8 +360,6 @@
     for i in TP_ORDER:
         copy_to(r_b.at[tp], r_b.at[tp], 6, (kv, tp_peer(i))).start()
     ld_mgain.wait()
-    ld_wg.wait()
-    ld_wu.wait()
     wait_bytes(r_b.at[pl.ds(0, N_TP - 1)], recv_sem.at[6, 0])
     branch = up(r_b[0])
     for i in range(1, N_TP):
@@ -363,14 +371,12 @@
         column_to_row(jnp.sum(residual * residual, axis=1, keepdims=True))
     )
 
-    across = (((1,), (1,)), ((), ()))
-    width = wg.shape[0]
     for j in range(CHUNKS):
         lo, hi = j * 128, min(j * 128 + 128, width)
         n = hi - lo
         at = iota((ROWS, n), 0)
-        g_j = lax.dot_general(normed_mid, wg[lo:hi, :], across, preferred_element_type=F32)
-        u_j = lax.dot_general(normed_mid, wu[lo:hi, :], across, preferred_element_type=F32)
+        g_j = jnp.dot(normed_mid, wg_t[j, :, 0:n], preferred_element_type=F32)
+        u_j = jnp.dot(normed_mid, wu_t[j, :, 0:n], preferred_element_type=F32)
         g_j = jnp.where(at == SEQS, sq_high[:, :n], jnp.where(at == SEQS + 1, sq_low[:, :n], g_j))
         b_g[j, 0:3, :, 0:n] = g_j.reshape(3, 8, n).astype(BF16)
         b_g[j, 3:6, :, 0:n] = u_j.reshape(3, 8, n).astype(BF16)
@@ -498,6 +504,8 @@
         vmem((N_TP, 16, 128), BF16),
         vmem((N_TP, 16, 128), BF16),
         vmem((seqs, dim, positions * heads), BF16),
+        vmem((CHUNKS, 128, 128), BF16),
+        vmem((CHUNKS, 128, 128), BF16),
         pltpu.SemaphoreType.DMA((len(args),)),
         pltpu.SemaphoreType.DMA((10,)),
         pltpu.SemaphoreType.DMA((10, N_Z)),

time: 61.9 us -> 61.7 us (level)
  no operation moved by 1% of the time
where the time goes in v3:
time: 61.7 us; the launch traced here: 61.6 us
  Pallas kernels  61 us (99%)
    pallas_call x1, Pallas kernels, per_device(): pl.pallas_call(kernel, out_shape=pltpu.VMEM((tokens.shape[1], seqs), BF16...  61 us

profile of v3, /device:TPU:1, one launch (start us, length us, event | category | flops | bytes accessed | tf_op | source)
XLA Modules:
  0.0 61.6 jit_solution(6092097763602964604)
XLA Ops:
  0.0 61.0 %decode_step.1 = bf16[16,22]{1,0:T(8,128)(2,1)S(1)} custom-call(bf16[16,22]{1,0:T(8,128)(2,1)} %bitcast.15, f32[1,128]{1,0:T(1,128)} %bitcast.16, bf16[128,512]{1,0:T(8,128)(2,1)} %wq_hbm.1, bf16[128,512]{1,0:T(8,128)(2,1)} %wk_hbm.1, bf16[128,512]{1,0:T(8,128)(2,1)} %wv_hbm.1, bf16[22,1024,128]{2,1,0:T(8,128)(2,1)} %bitcast.11, ...), custom_call_target="tpu_custom_call" | custom-call | tf_op jit(solution)/shard_map/decode_step/pallas_call | solution.py:513
  61.0 0.6 copy.16
